TPU v7x, 32 devices: a whole 2x2x4 slice. The times are simulated.
32 devices in a mesh: sp: 16 (over z, y, x), tp: 2 (over core).
Axes of the slice: x: 2, y: 2, z: 4, core: 2. Of those that a mesh axis runs over, the one named last changes fastest.
Arguments:
- tokens: bfloat16 [3072, 4096], P('sp'), may hold values from -6 to 6
- norm_gain: float32 [4096], replicated, may hold values from 0.1 to 1.9
- conv_value: bfloat16 [4096, 2048], P('sp', 'tp'), may hold values from -0.09375 to 0.09375
- conv_gate: bfloat16 [4096, 2048], P('sp', 'tp'), may hold values from -0.09375 to 0.09375
- state_feed: bfloat16 [4096, 2048], P('sp', 'tp'), may hold values from -0.09375 to 0.09375
- conv_taps: float32 [31, 2048], P(None, 'tp'), may hold values from -1 to 1
- chan_gain: float32 [2048], replicated, may hold values from 0.1 to 1.9
- chan_shift: float32 [2048], replicated, may hold values from -3 to 3
- conv_project: bfloat16 [2048, 4096], P('sp', 'tp'), may hold values from -0.125 to 0.125
- decay_rate: float32 [128, 64], P('tp'), may hold values from 0.1 to 3
- frequency: float32 [128, 64], P('tp'), may hold values from 0.1 to 3
- input_real: float32 [128, 64, 16], P('tp'), may hold values from -0.0390625 to 0.0390625
- input_imag: float32 [128, 64, 16], P('tp'), may hold values from -0.0390625 to 0.0390625
- output_real: float32 [128, 16, 64], P('tp'), may hold values from -0.5 to 0.5
- output_imag: float32 [128, 16, 64], P('tp'), may hold values from -0.5 to 0.5
- skip_gain: float32 [2048], P('tp'), may hold values from -3 to 3
- state_value: bfloat16 [2048, 4096], P('sp', 'tp'), may hold values from -0.125 to 0.125
- state_gate: bfloat16 [2048, 4096], P('sp', 'tp'), may hold values from -0.125 to 0.125
- initial_state: float32 [2, 128, 64], P(None, 'tp'), may hold values from -5 to 5
Outputs:
- mixer_out: bfloat16 [3072, 4096], P('sp', 'tp')
- final_state: float32 [2, 128, 64], P(None, 'tp')
All inputs are finite; a program needn't handle non-finite values.
Results may differ from a plain program's by a relative error of at most 0.0085.
Values may be sent and summed in bfloat16 or wider, within the bound.
A program may use at most 128 MiB of HBM per device.

v0:
```python
import jax
import jax.numpy as jnp
from jax import lax
from jax.sharding import PartitionSpec as P


def passed_along(value, axis, steps):
    count = lax.axis_size(axis)
    leading, last = (max(0, -steps), min(count, count - steps))
    return lax.ppermute(value, axis, [(source, source + steps) for source in range(leading, last)])


def rotate(first_real, first_imag, second_real, second_imag):
    return (
        first_real * second_real - first_imag * second_imag,
        first_real * second_imag + first_imag * second_real,
    )


def power_table(base_real, base_imag, exponent, largest):
    result_real = jnp.ones((exponent.shape[0], base_real.shape[0]), jnp.float32)
    result_imag = jnp.zeros((exponent.shape[0], base_real.shape[0]), jnp.float32)
    square_real, square_imag = (base_real, base_imag)
    for place in range(max(largest, 1).bit_length()):
        chosen = (exponent >> place & 1 == 1)[:, None]
        next_real, next_imag = rotate(result_real, result_imag, square_real, square_imag)
        result_real = jnp.where(chosen, next_real, result_real)
        result_imag = jnp.where(chosen, next_imag, result_imag)
        square_real, square_imag = rotate(square_real, square_imag, square_real, square_imag)
    return (result_real, result_imag)


def local(
    tokens,
    norm_gain,
    conv_value,
    conv_gate,
    state_feed,
    conv_taps,
    chan_gain,
    chan_shift,
    conv_project,
    decay_rate,
    frequency,
    input_real,
    input_imag,
    output_real,
    output_imag,
    skip_gain,
    state_value,
    state_gate,
    initial_state,
):
    highest = lax.Precision.HIGHEST
    floats = tokens.astype(jnp.float32)
    normed = (
        floats * lax.rsqrt(jnp.mean(floats * floats, axis=1, keepdims=True) + 1e-06) * norm_gain
    ).astype(jnp.bfloat16)
    length = tokens.shape[0]
    width = conv_value.shape[1]
    in_block = jnp.concatenate([conv_value, conv_gate, state_feed], axis=1)
    projected = jnp.dot(
        normed,
        lax.all_gather(in_block, "sp", axis=0, tiled=True),
        preferred_element_type=jnp.float32,
    )
    gated_linear = (projected[:, :width] * jax.nn.sigmoid(projected[:, width : 2 * width])).astype(
        jnp.bfloat16
    )
    state_drive = projected[:, 2 * width :].astype(jnp.bfloat16)
    kernel = conv_taps.shape[0]
    before = passed_along(gated_linear[length - (kernel - 1) :], "sp", 1)
    padded = jnp.concatenate([before, gated_linear], axis=0).astype(jnp.float32)
    conv_sum = jnp.zeros((length, width), jnp.float32)
    for offset in range(kernel):
        conv_sum = conv_sum + conv_taps[offset] * padded[offset : offset + length]
    conv_out = conv_sum.astype(jnp.bfloat16)
    seq_devices = lax.axis_size("sp")
    total_tokens = length * seq_devices
    groups, state_size, group_size = input_real.shape
    flat = groups * state_size
    rate_real = -decay_rate / total_tokens
    magnitude = jnp.exp(rate_real)
    step_real = magnitude * jnp.cos(frequency)
    step_imag = magnitude * jnp.sin(frequency)
    modulus = rate_real * rate_real + frequency * frequency
    lift_real = step_real - 1.0
    factor_real = (lift_real * rate_real + step_imag * frequency) / modulus
    factor_imag = (step_imag * rate_real - lift_real * frequency) / modulus
    drive_real = factor_real[..., None] * input_real - factor_imag[..., None] * input_imag
    drive_imag = factor_real[..., None] * input_imag + factor_imag[..., None] * input_real
    grouped = state_drive.astype(jnp.float32).reshape(length, groups, group_size)
    pushed_real = jnp.einsum("gph,tgh->tgp", drive_real, grouped, precision=highest).reshape(
        length, flat
    )
    pushed_imag = jnp.einsum("gph,tgh->tgp", drive_imag, grouped, precision=highest).reshape(
        length, flat
    )
    base_real = step_real.reshape(flat)
    base_imag = step_imag.reshape(flat)
    square_size = base_real * base_real + base_imag * base_imag
    back_real = base_real / square_size
    back_imag = -base_imag / square_size
    positions = lax.iota(jnp.int32, length)
    counted = positions + 1
    power_real, power_imag = power_table(base_real, base_imag, counted, length)
    undo_real, undo_imag = power_table(back_real, back_imag, counted, length)
    scaled_real, scaled_imag = rotate(undo_real, undo_imag, pushed_real, pushed_imag)
    lower = (positions[:, None] >= positions[None, :]).astype(jnp.float32)
    summed_real = jnp.dot(lower, scaled_real, precision=highest)
    summed_imag = jnp.dot(lower, scaled_imag, precision=highest)
    local_real, local_imag = rotate(power_real, power_imag, summed_real, summed_imag)
    span_real, span_imag = (power_real[-1], power_imag[-1])
    last_real, last_imag = (local_real[-1], local_imag[-1])
    start_real = initial_state[0].reshape(flat)
    start_imag = initial_state[1].reshape(flat)
    finals = lax.all_gather(jnp.stack([last_real, last_imag])[None], "sp", axis=0, tiled=True)
    position = lax.axis_index("sp")
    device_ids = lax.iota(jnp.int32, seq_devices)
    lag = jnp.maximum(position - 1 - device_ids, 0)
    weight_real, weight_imag = power_table(span_real, span_imag, lag, seq_devices)
    before_mask = (device_ids < position).astype(jnp.float32)[:, None]
    moved_real, moved_imag = rotate(weight_real, weight_imag, finals[:, 0], finals[:, 1])
    lead_real, lead_imag = power_table(
        span_real, span_imag, jnp.stack([position, jnp.int32(seq_devices)]), seq_devices
    )
    opening_real, opening_imag = rotate(lead_real[0], lead_imag[0], start_real, start_imag)
    entry_real = opening_real + jnp.sum(moved_real * before_mask, axis=0)
    entry_imag = opening_imag + jnp.sum(moved_imag * before_mask, axis=0)
    tail_real, tail_imag = power_table(
        span_real, span_imag, seq_devices - 1 - device_ids, seq_devices
    )
    carried_real, carried_imag = rotate(tail_real, tail_imag, finals[:, 0], finals[:, 1])
    closing_real, closing_imag = rotate(lead_real[1], lead_imag[1], start_real, start_imag)
    final_real = closing_real + jnp.sum(carried_real, axis=0)
    final_imag = closing_imag + jnp.sum(carried_imag, axis=0)
    final_state = jnp.stack([final_real, final_imag]).reshape(2, groups, state_size)
    state_real = (power_real * entry_real - power_imag * entry_imag + local_real).reshape(
        length, groups, state_size
    )
    state_imag = (power_real * entry_imag + power_imag * entry_real + local_imag).reshape(
        length, groups, state_size
    )
    response = jnp.einsum("ghp,tgp->tgh", output_real, state_real, precision=highest) - jnp.einsum(
        "ghp,tgp->tgh", output_imag, state_imag, precision=highest
    )
    response = response.reshape(length, groups * group_size) + skip_gain * state_drive.astype(
        jnp.float32
    )
    activated = jax.nn.gelu(response).astype(jnp.bfloat16)
    conv_rows, activated_rows = (
        lax.all_gather(conv_out, "tp", axis=1, tiled=True),
        lax.all_gather(activated, "tp", axis=1, tiled=True),
    )
    conv_full = conv_rows.astype(jnp.float32)
    row_mean = jnp.mean(conv_full, axis=1, keepdims=True)
    centred = conv_full - row_mean
    variance = jnp.mean(centred * centred, axis=1, keepdims=True)
    conv_act = jax.nn.silu(centred * lax.rsqrt(variance + 1e-05) * chan_gain + chan_shift).astype(
        jnp.bfloat16
    )
    columns = conv_project.shape[1]
    out_block = jnp.concatenate([conv_project, state_value, state_gate], axis=1)
    piece = lax.all_gather(out_block, "sp", axis=0, tiled=True)
    conv_branch = jnp.dot(conv_act, piece[:, :columns], preferred_element_type=jnp.float32)
    state_both = jnp.dot(activated_rows, piece[:, columns:], preferred_element_type=jnp.float32)
    mixer_out = (
        conv_branch + state_both[:, :columns] * jax.nn.sigmoid(state_both[:, columns:])
    ).astype(jnp.bfloat16)
    return (mixer_out, final_state)


def solution(mesh):
    in_specs = (
        P("sp", None),
        P(),
        P("sp", "tp"),
        P("sp", "tp"),
        P("sp", "tp"),
        P(None, "tp"),
        P(),
        P(),
        P("sp", "tp"),
        P("tp", None),
        P("tp", None),
        P("tp", None, None),
        P("tp", None, None),
        P("tp", None, None),
        P("tp", None, None),
        P("tp"),
        P("sp", "tp"),
        P("sp", "tp"),
        P(None, "tp", None),
    )
    out_specs = (P("sp", "tp"), P(None, "tp", None))
    return jax.shard_map(local, mesh=mesh, in_specs=in_specs, out_specs=out_specs, check_vma=False)
```

profile of v0, /device:TPU:0, one launch (start us, length us, event | category | flops | bytes accessed | tf_op | source)
XLA Modules:
  0.0 595.5 jit_solution(7668564235694734183)
XLA Ops:
  7.2 2.7 pad_maximum_fusion
  10.1 2.4 pad_maximum_fusion.1
  12.5 0.2 sine_multiply_fusion
  12.9 0.1 reshape_squeeze.6
  12.9 0.1 reshape_squeeze.7
  13.3 0.4 fusion.4
  13.8 7.6 %add_select_fusion.5 = f32[192,4096]{1,0:T(8,128)S(1)} fusion(f32[4096]{0:T(1024)S(1)} %get-tuple-element.123, f32[4096]{0:T(1024)S(1)} %get-tuple-element.122, pred[192]{0:T(512)(128)(4,1)S(1)} %get-tuple-element.135, f32[4096]{0:T(1024)S(1)} %get-tuple-element.125, f32[4096]{0:T(1024)S(1)} %get-tuple-element.124, f32[4096]{0:T(1024)S(1)} %get-tuple-element.126, ...), kind=kLoop, calls=%fused_computation.63 | loop fusion | flops 42467328 | bytes 3409408 | tf_op jit(solution)/shard_map/jit(_where)/select_n | solution.py:28
  21.4 7.7 %subtract_select_fusion.5 = f32[192,4096]{1,0:T(8,128)S(1)} fusion(f32[4096]{0:T(1024)S(1)} %get-tuple-element.123, f32[4096]{0:T(1024)S(1)} %get-tuple-element.122, pred[192]{0:T(512)(128)(4,1)S(1)} %get-tuple-element.135, f32[4096]{0:T(1024)S(1)} %get-tuple-element.125, f32[4096]{0:T(1024)S(1)} %get-tuple-element.124, f32[4096]{0:T(1024)S(1)} %get-tuple-element.126, ...), kind=kLoop, calls=%fused_computation.64 | loop fusion | flops 42467328 | bytes 3409408 | tf_op jit(solution)/shard_map/jit(_where)/select_n | solution.py:27
  29.1 0.1 multiply_subtract_fusion.9
  29.4 0.2 add_select_fusion.16
  29.6 0.1 subtract_select_fusion.14
  29.8 254.3 %all-gather.5.cloned.1.call-done = bf16[4096,3072]{1,0:T(8,128)(2,1)} async-done(((bf16[256,3072]{1,0:T(8,128)(2,1)}), bf16[4096,3072]{1,0:T(8,128)(2,1)}) %all-gather.5.cloned.1.call-update) | async-done | bytes 25165840 | tf_op jit(solution)/shard_map/all_gather | solution.py:64
  284.1 11.3 %fusion.52 = f32[192,3072]{1,0:T(8,128)S(1)} fusion(bf16[4096,3072]{1,0:T(8,128)(2,1)} %all-gather.5.cloned.1.call-done, bf16[192,4096]{1,0:T(8,128)(2,1)} %param.19, f32[4096]{0:T(1024)S(1)} %copy-done.18, f32[192]{0:T(256)S(1)} %add_rsqrt_fusion.1), kind=kOutput, calls=%fused_computation.88 | convolution fusion | flops 4834983936 | bytes 29115136 | tf_op jit(solution)/shard_map/dot_general | solution.py:62
  295.4 1.4 copy-done.6
  296.8 0.2 copy.40
  297.0 3.9 fusion.114
  300.9 5.3 copy.41
  306.2 3.8 fusion.110
  310.1 5.5 copy.42
  315.6 11.8 %fusion.31 = f32[192,4096]{1,0:T(8,128)S(1)} fusion(f32[192,4096]{1,0:T(8,128)} %copy.42, f32[192,4096]{1,0:T(8,128)} %copy.41, f32[4096]{0:T(1024)S(1)} %get-tuple-element.110, f32[4096]{0:T(1024)S(1)} %get-tuple-element.109, pred[192]{0:T(512)(128)(4,1)S(1)} %get-tuple-element.135, f32[4096]{0:T(1024)S(1)} %get-tuple-element.112, ...), kind=kOutput, calls=%fused_computation.49 | convolution fusion | flops 1859948544 | bytes 9700864 | tf_op jit(solution)/shard_map/dot_general | solution.py:110
  327.4 16.5 %multiply_subtract_fusion = (f32[192,4096]{1,0:T(8,128)S(1)}, f32[192,4096]{1,0:T(8,128)S(1)}) fusion(f32[192,4096]{1,0:T(8,128)S(1)} %fusion.31, f32[4096]{0:T(1024)S(1)} %get-tuple-element.123, f32[4096]{0:T(1024)S(1)} %get-tuple-element.122, f32[4096]{0:T(1024)S(1)} %get-tuple-element.125, f32[4096]{0:T(1024)S(1)} %get-tuple-element.124, ...), kind=kOutput, calls=%fused_computation.44 | convolution fusion | flops 1907920896 | bytes 16254464 | tf_op jit(solution)/shard_map/dot_general | solution.py:111
  343.9 8.0 %multiply_add_fusion = f32[192,4096]{1,0:T(8,128)S(1)} fusion(f32[192,4096]{1,0:T(8,128)S(1)} %fusion.31, f32[192,4096]{1,0:T(8,128)S(1)} %get-tuple-element.119, f32[4096]{0:T(1024)S(1)} %get-tuple-element.123, f32[4096]{0:T(1024)S(1)} %get-tuple-element.122, f32[4096]{0:T(1024)S(1)} %get-tuple-element.125, f32[4096]{0:T(1024)S(1)} %get-tuple-element.124, ...), kind=kLoop, calls=%fused_computation.43 | loop fusion | flops 47972352 | bytes 9700864 | tf_op jit(solution)/shard_map/add | solution.py:16
  352.0 1.6 copy-done.2
  353.7 45.9 %all-gather.1 = f32[16,2,4096]{2,1,0:T(2,128)S(1)} all-gather(f32[1,2,4096]{2,1,0:T(2,128)S(1)} %maximum_bitcast_fusion), channel_id=2, replica_groups=mesh['sp'=16,'tp'=2] {'sp'}, dimensions={0}, use_global_device_ids=true | all-gather | bytes 557056 | tf_op jit(solution)/shard_map/all_gather | solution.py:117
  399.7 0.5 fusion.166
  400.2 0.6 fusion.145
  400.9 0.7 fusion.140
  401.5 0.2 add_reduce_fusion.1
  401.8 10.9 %add_add_fusion = f32[192,4096]{1,0:T(8,128)} fusion(f32[192,4096]{1,0:T(8,128)} %copy-done.2, f32[4096]{0:T(1024)S(1)} %bitcast.138, f32[4096]{0:T(1024)S(1)} %bitcast.140, f32[4096]{0:T(1024)S(1)} %get-tuple-element.123, f32[4096]{0:T(1024)S(1)} %get-tuple-element.122, f32[4096]{0:T(1024)S(1)} %get-tuple-element.125, f32[4096]{0:T(1024)S(1)} %get-tuple-element.124, ...), kind=kLoop, calls=%fused_computation.41 | loop fusion | flops 48758784 | bytes 6587904 | tf_op jit(solution)/shard_map/add | solution.py:141
  412.8 5.2 copy.47
  417.9 10.8 %subtract_add_fusion = f32[192,4096]{1,0:T(8,128)} fusion(f32[192,4096]{1,0:T(8,128)} %copy-done.3, f32[4096]{0:T(1024)S(1)} %bitcast.139, f32[4096]{0:T(1024)S(1)} %bitcast.141, f32[4096]{0:T(1024)S(1)} %get-tuple-element.123, f32[4096]{0:T(1024)S(1)} %get-tuple-element.122, f32[4096]{0:T(1024)S(1)} %get-tuple-element.125, f32[4096]{0:T(1024)S(1)} %get-tuple-element.124, ...), kind=kLoop, calls=%fused_computation.42 | loop fusion | flops 48758784 | bytes 6587904 | tf_op jit(solution)/shard_map/add | solution.py:138
  428.7 5.5 copy.46
  434.2 4.6 fusion.170
  438.8 2.4 convolution_subtract_fusion
  441.2 0.3 copy.48
  441.5 1.6 fusion.109
  443.1 1.5 collective-permute-start
  444.6 1.4 fusion.68
  446.1 2.4 all_gather.19
  448.5 118.7 %all-gather.7.cloned.1.call-done = bf16[2048,6144]{1,0:T(8,128)(2,1)} async-done(((bf16[128,6144]{1,0:T(8,128)(2,1)}), bf16[2048,6144]{1,0:T(8,128)(2,1)}) %all-gather.7.cloned.1.call-update) | async-done | bytes 25165840 | tf_op jit(solution)/shard_map/all_gather | solution.py:164
  567.2 7.6 %fusion = f32[192,4096]{1,0:T(8,128)S(1)} fusion(bf16[192,2048]{1,0:T(8,128)(2,1)S(1)} %all_gather.19, bf16[2048,6144]{1,0:T(8,128)(2,1)} %all-gather.7.cloned.1.call-done), kind=kOutput, calls=%fused_computation | convolution fusion | flops 3221225472 | bytes 20709376 | tf_op jit(solution)/shard_map/dot_general | solution.py:166
  574.8 0.6 pad_maximum_fusion.2
  575.4 0.1 maximum_convert_fusion
  575.5 3.1 fusion.70
  578.6 2.4 all_gather.16
  581.0 0.2 convert_reduce_fusion
  581.2 0.4 fusion.43
  581.6 6.6 %fusion.38 = bf16[192,2048]{1,0:T(8,128)(2,1)} fusion(bf16[2048,6144]{1,0:T(8,128)(2,1)} %all-gather.7.cloned.1.call-done, f32[192,4096]{1,0:T(8,128)S(1)} %fusion, bf16[192,2048]{1,0:T(8,128)(2,1)S(1)} %all_gather.16, f32[2048]{0:T(1024)S(1)} %copy-done.19, f32[2048]{0:T(1024)S(1)} %copy-done.20, f32[192]{0:T(256)S(1)} %add_rsqrt_fusion, ...), kind=kOutput, calls=%fused_computation.74 | convolution fusion | flops 1616904192 | bytes 13125120 | tf_op jit(solution)/shard_map/dot_general | solution.py:165
  (80 shorter events, 1.2 us)
Async XLA Ops:
  7.2 427.0 %copy-start = (f32[64,16,64]{2,1,0:T(8,128)S(1)}, f32[64,16,64]{2,1,0:T(8,128)}, u32[]{:S(2)}) copy-start(f32[64,16,64]{2,1,0:T(8,128)} %param.32) | copy-start | bytes 786436
  7.2 2.9 copy-start.11
  7.2 2.9 copy-start.10
  7.2 276.9 %all-gather.5.cloned.1.call-start = ((), (), s32[]{:S(2)}) async-start(), calls=%async_computation | async-start | bytes 26738688 | tf_op jit(solution)/shard_map/all_gather | solution.py:64
  10.0 2.6 copy-start.15
  10.0 2.6 copy-start.16
  10.0 2.9 copy-start.14
  10.0 3.3 copy-start.9
  10.0 557.1 %all-gather.7.cloned.1.call-start = ((), (), s32[]{:S(2)}) async-start(), calls=%async_computation.1 | async-start | bytes 26738688 | tf_op jit(solution)/shard_map/all_gather | solution.py:164
  13.8 15.5 %copy-start.13 = (f32[31,1024]{1,0:T(8,128)S(1)}, f32[31,1024]{1,0:T(8,128)}, u32[]{:S(2)}) copy-start(f32[31,1024]{1,0:T(8,128)} %param.24) | copy-start | bytes 380932
  21.3 262.7 %copy-start.18 = (f32[4096]{0:T(1024)S(1)}, f32[4096]{0:T(1024)}, u32[]{:S(2)}) copy-start(f32[4096]{0:T(1024)} %param.20) | copy-start | bytes 49156
  29.8 267.2 %copy-start.7 = (f32[64,64,16]{1,2,0:T(8,128)S(1)}, f32[64,64,16]{1,2,0:T(8,128)}, u32[]{:S(2)}) copy-start(f32[64,64,16]{1,2,0:T(8,128)} %param.30) | copy-start | bytes 786436
  29.8 267.2 %copy-start.8 = (f32[64,64,16]{1,2,0:T(8,128)S(1)}, f32[64,64,16]{1,2,0:T(8,128)}, u32[]{:S(2)}) copy-start(f32[64,64,16]{1,2,0:T(8,128)} %param.31) | copy-start | bytes 786436
  295.4 1.4 copy-start.6
  315.6 11.8 %copy-start.4 = (f32[192,4096]{1,0:T(8,128)S(1)}, f32[192,4096]{1,0:T(8,128)}, u32[]{:S(2)}) copy-start(f32[192,4096]{1,0:T(8,128)} %copy.41) | copy-start | bytes 9437188
  315.6 11.8 %copy-start.5 = (f32[192,4096]{1,0:T(8,128)S(1)}, f32[192,4096]{1,0:T(8,128)}, u32[]{:S(2)}) copy-start(f32[192,4096]{1,0:T(8,128)} %copy.42) | copy-start | bytes 9437188
  343.9 9.7 %copy-start.3 = (f32[192,4096]{1,0:T(8,128)}, f32[192,4096]{1,0:T(8,128)S(1)}, u32[]{:S(2)}) copy-start(f32[192,4096]{1,0:T(8,128)S(1)} %get-tuple-element.118) | copy-start | bytes 9437188
  352.0 1.7 copy-start.2
  434.2 4.6 copy-start.1
  434.2 4.6 copy-start.12
  441.2 3.5 copy-start.17
  443.1 132.3 %collective-permute-start = (bf16[30,1024]{1,0:T(8,128)(2,1)S(1)}, bf16[30,1024]{1,0:T(8,128)(2,1)S(1)}, u32[]{:S(2)}, u32[]{:S(2)}) collective-permute-start(bf16[30,1024]{1,0:T(8,128)(2,1)S(1)} %slice.333), channel_id=1, source_target_pairs={{0,2},{2,4},{4,6},{6,8},{8,10},{10,12},{12,14},{14,16},{16,18},{18... | collective-permute-start | bytes 184328 | tf_op jit(solution)/shard_map/ppermute | solution.py:10
  575.5 6.0 %copy-start.19 = (f32[2048]{0:T(1024)S(1)}, f32[2048]{0:T(1024)}, u32[]{:S(2)}) copy-start(f32[2048]{0:T(1024)} %param.26) | copy-start | bytes 24580
  575.5 6.0 %copy-start.20 = (f32[2048]{0:T(1024)S(1)}, f32[2048]{0:T(1024)}, u32[]{:S(2)}) copy-start(f32[2048]{0:T(1024)} %param.25) | copy-start | bytes 24580
Sparse Core Ops, SparseCore 0:
  10.8 273.2 all-gather.4
  286.8 280.2 all-gather.6
where the time goes:
time: 605 us; the launch traced here: 595 us
  waiting for transfers between devices  373 us (62%)
  matrix products  68.4 us (11%)
  other arithmetic  60.4 us (10%)
  blocking collectives  50.7 us (8%)
  local copies, waits for them, and re-layouts  26.3 us (4%)
  between operations  15.1 us (2%)
    all_gather x1, waiting for transfers between devices, local(): lax.all_gather(in_block, 'sp', axis=0, tiled=True)  254 us
    all_gather x1, waiting for transfers between devices, local(): piece = lax.all_gather(out_block, 'sp', axis=0, tiled=True)  119 us
    all_gather x1, blocking collectives, local(): lax.all_gather(jnp.stack([last_real, last_imag])[None], 'sp', axis=0, til...  45.9 us
    dot_general x1, matrix products, local(): summed_imag = jnp.dot(lower, scaled_imag, precision=highest)  16.5 us
  transfers between devices with their start and end apart: 3, of which 2 were waited for; matrix products, arithmetic and copies ran while one was open for 23% of the time, Pallas kernels for 0%

commit v1 on v0

--- a/solution.py
+++ b/solution.py
@@ -161,7 +161,12 @@
     )
     columns = conv_project.shape[1]
     out_block = jnp.concatenate([conv_project, state_value, state_gate], axis=1)
-    piece = lax.all_gather(out_block, "sp", axis=0, tiled=True)
+    ring = [out_block]
+    for hop in range(15):
+        ring.append(lax.ppermute(ring[-1], "sp", [(dev, (dev + 1) % 16) for dev in range(16)]))
+    piece = jnp.roll(
+        jnp.concatenate(ring[::-1], axis=0), (lax.axis_index("sp") + 1) * ring[0].shape[0], axis=0
+    )
     conv_branch = jnp.dot(conv_act, piece[:, :columns], preferred_element_type=jnp.float32)
     state_both = jnp.dot(activated_rows, piece[:, columns:], preferred_element_type=jnp.float32)
     mixer_out = (

time: 605 us -> 1020 us (1.69)
  waiting for transfers between devices: 373 us -> 720 us
  local copies, waits for them, and re-layouts: 26.3 us -> 91.4 us
    ppermute x0 -> x15, waiting for transfers between devices: none -> 720 us  [local(): lax.ppermute(ring[-1], 'sp', [(dev, (dev + 1) % 16) for dev in range(16)])]
    all_gather x1, waiting for transfers between devices: 254 us -> 0.01 us  [local(): lax.all_gather(in_block, 'sp', axis=0, tiled=True)]
    all_gather x1 -> x0, waiting for transfers between devices: 119 us -> none  [local(): piece = lax.all_gather(out_block, 'sp', axis=0, tiled=True)]
    unnamed x42 -> x347, local copies, waits for them, and re-layouts: 3.11 us -> 63.3 us
  transfers between devices with their start and end apart: 3 -> 17, of which waited for: 2 -> 15; matrix products, arithmetic and copies ran while one was open for 23% -> 9% of each run, Pallas kernels for 0% -> 0%
where the time goes in v1:
time: 1020 us
  waiting for transfers between devices  720 us (71%)
  local copies, waits for them, and re-layouts  91.4 us (9%)
  matrix products  69.4 us (7%)
  other arithmetic  68.4 us (7%)
  blocking collectives  43 us (4%)
  between operations  16.4 us (2%)
    ppermute x15, waiting for transfers between devices, local(): lax.ppermute(ring[-1], 'sp', [(dev, (dev + 1) % 16) for dev in range(16)])  720 us
    unnamed x347, local copies, waits for them, and re-layouts  63.3 us
    all_gather x1, blocking collectives, local(): lax.all_gather(jnp.stack([last_real, last_imag])[None], 'sp', axis=0, til...  38.3 us
  transfers between devices with their start and end apart: 17, of which 15 were waited for; matrix products, arithmetic and copies ran while one was open for 9% of the time, Pallas kernels for 0%

profile of v1, /device:TPU:0, one launch (start us, length us, event | category | flops | bytes accessed | tf_op | source)
XLA Modules:
  0.0 1016.2 jit_solution(14925743718559360550)
XLA Ops:
  7.3 2.8 pad_maximum_fusion.1
  10.1 3.0 collective-permute-start.1
  14.4 58.4 %collective-permute-done.1 = bf16[128,6144]{1,0:T(8,128)(2,1)S(1)} collective-permute-done((bf16[128,6144]{1,0:T(8,128)(2,1)}, bf16[128,6144]{1,0:T(8,128)(2,1)S(1)}, u32[]{:S(2)}, u32[]{:S(2)}) %collective-permute-start.1) | collective-permute-done | bytes 1572896 | tf_op jit(solution)/shard_map/ppermute | solution.py:166
  72.8 65.4 %collective-permute-done.2 = bf16[128,6144]{1,0:T(8,128)(2,1)S(1)} collective-permute-done((bf16[128,6144]{1,0:T(8,128)(2,1)S(1)}, bf16[128,6144]{1,0:T(8,128)(2,1)S(1)}, u32[]{:S(2)}, u32[]{:S(2)}) %collective-permute-start.2) | collective-permute-done | bytes 1572896 | tf_op jit(solution)/shard_map/ppermute | solution.py:166
  139.4 73.2 %collective-permute-done.3 = bf16[128,6144]{1,0:T(8,128)(2,1)S(1)} collective-permute-done((bf16[128,6144]{1,0:T(8,128)(2,1)S(1)}, bf16[128,6144]{1,0:T(8,128)(2,1)S(1)}, u32[]{:S(2)}, u32[]{:S(2)}) %collective-permute-start.3) | collective-permute-done | bytes 1572896 | tf_op jit(solution)/shard_map/ppermute | solution.py:166
  213.8 62.9 %collective-permute-done.4 = bf16[128,6144]{1,0:T(8,128)(2,1)S(1)} collective-permute-done((bf16[128,6144]{1,0:T(8,128)(2,1)S(1)}, bf16[128,6144]{1,0:T(8,128)(2,1)S(1)}, u32[]{:S(2)}, u32[]{:S(2)}) %collective-permute-start.4) | collective-permute-done | bytes 1572896 | tf_op jit(solution)/shard_map/ppermute | solution.py:166
  277.8 72.8 %collective-permute-done.5 = bf16[128,6144]{1,0:T(8,128)(2,1)S(1)} collective-permute-done((bf16[128,6144]{1,0:T(8,128)(2,1)S(1)}, bf16[128,6144]{1,0:T(8,128)(2,1)S(1)}, u32[]{:S(2)}, u32[]{:S(2)}) %collective-permute-start.5) | collective-permute-done | bytes 1572896 | tf_op jit(solution)/shard_map/ppermute | solution.py:166
  351.8 72.5 %collective-permute-done.6 = bf16[128,6144]{1,0:T(8,128)(2,1)S(1)} collective-permute-done((bf16[128,6144]{1,0:T(8,128)(2,1)S(1)}, bf16[128,6144]{1,0:T(8,128)(2,1)S(1)}, u32[]{:S(2)}, u32[]{:S(2)}) %collective-permute-start.6) | collective-permute-done | bytes 1572896 | tf_op jit(solution)/shard_map/ppermute | solution.py:166
  425.4 64.6 %collective-permute-done.7 = bf16[128,6144]{1,0:T(8,128)(2,1)S(1)} collective-permute-done((bf16[128,6144]{1,0:T(8,128)(2,1)S(1)}, bf16[128,6144]{1,0:T(8,128)(2,1)S(1)}, u32[]{:S(2)}, u32[]{:S(2)}) %collective-permute-start.7) | collective-permute-done | bytes 1572896 | tf_op jit(solution)/shard_map/ppermute | solution.py:166
  491.2 37.8 %collective-permute-done.8 = bf16[128,6144]{1,0:T(8,128)(2,1)} collective-permute-done((bf16[128,6144]{1,0:T(8,128)(2,1)S(1)}, bf16[128,6144]{1,0:T(8,128)(2,1)}, u32[]{:S(2)}, u32[]{:S(2)}) %collective-permute-start.8) | collective-permute-done | bytes 1572896 | tf_op jit(solution)/shard_map/ppermute | solution.py:166
  533.1 33.0 %collective-permute-done.9 = bf16[128,6144]{1,0:T(8,128)(2,1)} collective-permute-done((bf16[128,6144]{1,0:T(8,128)(2,1)}, bf16[128,6144]{1,0:T(8,128)(2,1)}, u32[]{:S(2)}, u32[]{:S(2)}) %collective-permute-start.9) | collective-permute-done | bytes 1572896 | tf_op jit(solution)/shard_map/ppermute | solution.py:166
  568.7 33.7 %collective-permute-done.10 = bf16[128,6144]{1,0:T(8,128)(2,1)S(1)} collective-permute-done((bf16[128,6144]{1,0:T(8,128)(2,1)}, bf16[128,6144]{1,0:T(8,128)(2,1)S(1)}, u32[]{:S(2)}, u32[]{:S(2)}) %collective-permute-start.10) | collective-permute-done | bytes 1572896 | tf_op jit(solution)/shard_map/ppermute | solution.py:166
  604.8 8.6 add_select_fusion.5
  613.4 25.5 %collective-permute-done.11 = bf16[128,6144]{1,0:T(8,128)(2,1)} collective-permute-done((bf16[128,6144]{1,0:T(8,128)(2,1)S(1)}, bf16[128,6144]{1,0:T(8,128)(2,1)}, u32[]{:S(2)}, u32[]{:S(2)}) %collective-permute-start.11) | collective-permute-done | bytes 1572896 | tf_op jit(solution)/shard_map/ppermute | solution.py:166
  641.6 7.5 subtract_select_fusion.5
  649.3 24.3 %collective-permute-done.12 = bf16[128,6144]{1,0:T(8,128)(2,1)} collective-permute-done((bf16[128,6144]{1,0:T(8,128)(2,1)}, bf16[128,6144]{1,0:T(8,128)(2,1)}, u32[]{:S(2)}, u32[]{:S(2)}) %collective-permute-start.12) | collective-permute-done | bytes 1572896 | tf_op jit(solution)/shard_map/ppermute | solution.py:166
  676.8 31.6 %collective-permute-done.13 = bf16[128,6144]{1,0:T(8,128)(2,1)S(1)} collective-permute-done((bf16[128,6144]{1,0:T(8,128)(2,1)}, bf16[128,6144]{1,0:T(8,128)(2,1)S(1)}, u32[]{:S(2)}, u32[]{:S(2)}) %collective-permute-start.13) | collective-permute-done | bytes 1572896 | tf_op jit(solution)/shard_map/ppermute | solution.py:166
  708.6 34.2 %collective-permute-done.14 = bf16[128,6144]{1,0:T(8,128)(2,1)S(1)} collective-permute-done((bf16[128,6144]{1,0:T(8,128)(2,1)S(1)}, bf16[128,6144]{1,0:T(8,128)(2,1)S(1)}, u32[]{:S(2)}, u32[]{:S(2)}) %collective-permute-start.14) | collective-permute-done | bytes 1572896 | tf_op jit(solution)/shard_map/ppermute | solution.py:166
  744.4 30.3 %collective-permute-done.15 = bf16[128,6144]{1,0:T(8,128)(2,1)S(1)} collective-permute-done((bf16[128,6144]{1,0:T(8,128)(2,1)S(1)}, bf16[128,6144]{1,0:T(8,128)(2,1)S(1)}, u32[]{:S(2)}, u32[]{:S(2)}) %collective-permute-start.15) | collective-permute-done | bytes 1572896 | tf_op jit(solution)/shard_map/ppermute | solution.py:166
  778.6 2.9 constant_dynamic-update-slice_fusion.28
  781.5 2.7 constant_dynamic-update-slice_fusion.27
  785.5 2.9 constant_dynamic-update-slice_fusion.25
  788.4 2.8 constant_dynamic-update-slice_fusion.24
  806.5 2.7 constant_dynamic-update-slice_fusion.12
  809.3 2.7 constant_dynamic-update-slice_fusion.11
  813.2 2.7 constant_dynamic-update-slice_fusion.9
  815.9 2.7 constant_dynamic-update-slice_fusion.8
  830.1 11.3 %fusion.52 = f32[192,3072]{1,0:T(8,128)S(1)} fusion(bf16[4096,3072]{1,0:T(8,128)(2,1)} %all-gather.4.cloned.1.call-done, bf16[192,4096]{1,0:T(8,128)(2,1)} %param.19, f32[4096]{0:T(1024)S(1)} %copy-done.153, f32[192]{0:T(256)S(1)} %copy-done.143), kind=kOutput, calls=%fused_computation.88 | convolution fusion | flops 4834983936 | bytes 29115136 | tf_op jit(solution)/shard_map/dot_general | solution.py:62
  843.6 5.1 fusion.110
  848.7 3.9 fusion.114
  852.6 5.3 copy.42
  858.1 5.7 copy.41
  864.1 11.7 %fusion.31 = f32[192,4096]{1,0:T(8,128)S(1)} fusion(f32[192,4096]{1,0:T(8,128)} %copy.42, f32[192,4096]{1,0:T(8,128)} %copy.41, f32[4096]{0:T(1024)S(1)} %copy-done.89, f32[4096]{0:T(1024)S(1)} %copy-done.88, pred[192]{0:T(512)(128)(4,1)S(1)} %copy-done.127, f32[4096]{0:T(1024)S(1)} %copy-done.91, f32[4096]{0:T(1024)S(1)} %copy-done.90, ...), kind=kOutput, calls=%fused_computation.49 | convolution fusion | flops 1859948544 | bytes 9700864 | tf_op jit(solution)/shard_map/dot_general | solution.py:110
  875.9 16.3 %multiply_subtract_fusion = (f32[192,4096]{1,0:T(8,128)S(1)}, f32[192,4096]{1,0:T(8,128)S(1)}) fusion(f32[192,4096]{1,0:T(8,128)S(1)} %fusion.31, f32[4096]{0:T(1024)S(1)} %copy-done.28, f32[4096]{0:T(1024)S(1)} %copy-done.26, f32[4096]{0:T(1024)S(1)} %copy-done.32, f32[4096]{0:T(1024)S(1)} %copy-done.30, f32[4096]{0:T(1024)S(1)} %copy-done.34, ...), kind=kOutput, calls=%fused_computation.44 | convolution fusion | flops 1907920896 | bytes 16254464 | tf_op jit(solution)/shard_map/dot_general | solution.py:111
  892.5 8.1 multiply_add_fusion
  900.7 38.3 %all-gather.1 = f32[16,2,4096]{2,1,0:T(2,128)S(1)} all-gather(f32[1,2,4096]{2,1,0:T(2,128)S(1)} %maximum_bitcast_fusion), channel_id=2, replica_groups=mesh['sp'=16,'tp'=2] {'sp'}, dimensions={0}, use_global_device_ids=true | all-gather | bytes 557056 | tf_op jit(solution)/shard_map/all_gather | solution.py:117
  941.8 9.8 subtract_add_fusion
  951.7 9.4 add_add_fusion
  962.0 5.2 copy.46
  967.2 5.1 copy.47
  972.3 4.5 fusion.171
  976.8 2.4 convolution_subtract_fusion
  981.1 2.4 all_gather.15
  983.5 3.9 collective-permute-start
  987.8 7.6 fusion
  996.5 3.1 fusion.70
  999.6 2.4 all_gather.13
  1002.6 6.6 fusion.38
  (413 shorter events, 67.5 us)
Async XLA Ops:
  7.2 965.2 %copy-start = (f32[64,16,64]{2,1,0:T(8,128)S(1)}, f32[64,16,64]{2,1,0:T(8,128)}, u32[]{:S(2)}) copy-start(f32[64,16,64]{2,1,0:T(8,128)} %param.32) | copy-start | bytes 786436
  7.2 822.9 %all-gather.4.cloned.1.call-start = ((), (), s32[]{:S(2)}) async-start(), calls=%async_computation | async-start | bytes 26738688 | tf_op jit(solution)/shard_map/all_gather | solution.py:64
  10.1 519.0 %copy-start.77 = (f32[64,64]{1,0:T(8,128)S(1)}, f32[64,64]{1,0:T(8,128)}, u32[]{:S(2)}) copy-start(f32[64,64]{1,0:T(8,128)} %param.29) | copy-start | bytes 49156
  10.1 519.0 %copy-start.78 = (f32[64,64]{1,0:T(8,128)S(1)}, f32[64,64]{1,0:T(8,128)}, u32[]{:S(2)}) copy-start(f32[64,64]{1,0:T(8,128)} %param.28) | copy-start | bytes 49156
  10.1 558.6 %copy-start.76 = (f32[2,64,64]{2,1,0:T(8,128)S(1)}, f32[2,64,64]{2,1,0:T(8,128)}, u32[]{:S(2)}) copy-start(f32[2,64,64]{2,1,0:T(8,128)} %param.37) | copy-start | bytes 98308
  10.1 62.8 %collective-permute-start.1 = (bf16[128,6144]{1,0:T(8,128)(2,1)}, bf16[128,6144]{1,0:T(8,128)(2,1)S(1)}, u32[]{:S(2)}, u32[]{:S(2)}) collective-permute-start(bf16[128,6144]{1,0:T(8,128)(2,1)} %pad_maximum_fusion.1), channel_id=1, source_target_pairs={{0,2},{2,4},{4,6},{6,8},{8,10},{10,12},{12,14},{14,16},{16,18},{18... | collective-permute-start | bytes 4718600 | tf_op jit(solution)/shard_map/ppermute | solution.py:166
  72.8 65.4 %collective-permute-start.2 = (bf16[128,6144]{1,0:T(8,128)(2,1)S(1)}, bf16[128,6144]{1,0:T(8,128)(2,1)S(1)}, u32[]{:S(2)}, u32[]{:S(2)}) collective-permute-start(bf16[128,6144]{1,0:T(8,128)(2,1)S(1)} %collective-permute-done.1), channel_id=1, source_target_pairs={{0,2},{2,4},{4,6},{6,8},{8,10},{10,12},{12,14},{14,16},{16,18},{18... | collective-permute-start | bytes 4718600 | tf_op jit(solution)/shard_map/ppermute | solution.py:166
  139.4 73.2 %collective-permute-start.3 = (bf16[128,6144]{1,0:T(8,128)(2,1)S(1)}, bf16[128,6144]{1,0:T(8,128)(2,1)S(1)}, u32[]{:S(2)}, u32[]{:S(2)}) collective-permute-start(bf16[128,6144]{1,0:T(8,128)(2,1)S(1)} %collective-permute-done.2), channel_id=1, source_target_pairs={{0,2},{2,4},{4,6},{6,8},{8,10},{10,12},{12,14},{14,16},{16,18},{18... | collective-permute-start | bytes 4718600 | tf_op jit(solution)/shard_map/ppermute | solution.py:166
  213.8 62.9 %collective-permute-start.4 = (bf16[128,6144]{1,0:T(8,128)(2,1)S(1)}, bf16[128,6144]{1,0:T(8,128)(2,1)S(1)}, u32[]{:S(2)}, u32[]{:S(2)}) collective-permute-start(bf16[128,6144]{1,0:T(8,128)(2,1)S(1)} %collective-permute-done.3), channel_id=1, source_target_pairs={{0,2},{2,4},{4,6},{6,8},{8,10},{10,12},{12,14},{14,16},{16,18},{18... | collective-permute-start | bytes 4718600 | tf_op jit(solution)/shard_map/ppermute | solution.py:166
  277.8 72.8 %collective-permute-start.5 = (bf16[128,6144]{1,0:T(8,128)(2,1)S(1)}, bf16[128,6144]{1,0:T(8,128)(2,1)S(1)}, u32[]{:S(2)}, u32[]{:S(2)}) collective-permute-start(bf16[128,6144]{1,0:T(8,128)(2,1)S(1)} %collective-permute-done.4), channel_id=1, source_target_pairs={{0,2},{2,4},{4,6},{6,8},{8,10},{10,12},{12,14},{14,16},{16,18},{18... | collective-permute-start | bytes 4718600 | tf_op jit(solution)/shard_map/ppermute | solution.py:166
  351.7 72.5 %collective-permute-start.6 = (bf16[128,6144]{1,0:T(8,128)(2,1)S(1)}, bf16[128,6144]{1,0:T(8,128)(2,1)S(1)}, u32[]{:S(2)}, u32[]{:S(2)}) collective-permute-start(bf16[128,6144]{1,0:T(8,128)(2,1)S(1)} %collective-permute-done.5), channel_id=1, source_target_pairs={{0,2},{2,4},{4,6},{6,8},{8,10},{10,12},{12,14},{14,16},{16,18},{18... | collective-permute-start | bytes 4718600 | tf_op jit(solution)/shard_map/ppermute | solution.py:166
  425.4 64.6 %collective-permute-start.7 = (bf16[128,6144]{1,0:T(8,128)(2,1)S(1)}, bf16[128,6144]{1,0:T(8,128)(2,1)S(1)}, u32[]{:S(2)}, u32[]{:S(2)}) collective-permute-start(bf16[128,6144]{1,0:T(8,128)(2,1)S(1)} %collective-permute-done.6), channel_id=1, source_target_pairs={{0,2},{2,4},{4,6},{6,8},{8,10},{10,12},{12,14},{14,16},{16,18},{18... | collective-permute-start | bytes 4718600 | tf_op jit(solution)/shard_map/ppermute | solution.py:166
  491.2 37.8 %collective-permute-start.8 = (bf16[128,6144]{1,0:T(8,128)(2,1)S(1)}, bf16[128,6144]{1,0:T(8,128)(2,1)}, u32[]{:S(2)}, u32[]{:S(2)}) collective-permute-start(bf16[128,6144]{1,0:T(8,128)(2,1)S(1)} %collective-permute-done.7), channel_id=1, source_target_pairs={{0,2},{2,4},{4,6},{6,8},{8,10},{10,12},{12,14},{14,16},{16,18},{18... | collective-permute-start | bytes 4718600 | tf_op jit(solution)/shard_map/ppermute | solution.py:166
  529.0 37.2 %collective-permute-start.9 = (bf16[128,6144]{1,0:T(8,128)(2,1)}, bf16[128,6144]{1,0:T(8,128)(2,1)}, u32[]{:S(2)}, u32[]{:S(2)}) collective-permute-start(bf16[128,6144]{1,0:T(8,128)(2,1)} %collective-permute-done.8), channel_id=1, source_target_pairs={{0,2},{2,4},{4,6},{6,8},{8,10},{10,12},{12,14},{14,16},{16,18},{18... | collective-permute-start | bytes 4718600 | tf_op jit(solution)/shard_map/ppermute | solution.py:166
  530.0 119.2 %copy-start.124 = (pred[192]{0:T(512)(128)(4,1)}, pred[192]{0:T(512)(128)(4,1)S(1)}, u32[]{:S(2)}) copy-start(pred[192]{0:T(512)(128)(4,1)S(1)} %get-tuple-element.134) | copy-start | bytes 580
  530.0 119.2 %copy-start.126 = (pred[192]{0:T(512)(128)(4,1)}, pred[192]{0:T(512)(128)(4,1)S(1)}, u32[]{:S(2)}) copy-start(pred[192]{0:T(512)(128)(4,1)S(1)} %get-tuple-element.135) | copy-start | bytes 580
  530.0 119.2 %copy-start.128 = (pred[192]{0:T(512)(128)(4,1)}, pred[192]{0:T(512)(128)(4,1)S(1)}, u32[]{:S(2)}) copy-start(pred[192]{0:T(512)(128)(4,1)S(1)} %get-tuple-element.128) | copy-start | bytes 580
  530.0 119.2 %copy-start.130 = (pred[192]{0:T(512)(128)(4,1)}, pred[192]{0:T(512)(128)(4,1)S(1)}, u32[]{:S(2)}) copy-start(pred[192]{0:T(512)(128)(4,1)S(1)} %get-tuple-element.129) | copy-start | bytes 580
  530.0 119.2 %copy-start.132 = (pred[192]{0:T(512)(128)(4,1)}, pred[192]{0:T(512)(128)(4,1)S(1)}, u32[]{:S(2)}) copy-start(pred[192]{0:T(512)(128)(4,1)S(1)} %get-tuple-element.130) | copy-start | bytes 580
  530.0 119.2 %copy-start.134 = (pred[192]{0:T(512)(128)(4,1)}, pred[192]{0:T(512)(128)(4,1)S(1)}, u32[]{:S(2)}) copy-start(pred[192]{0:T(512)(128)(4,1)S(1)} %get-tuple-element.131) | copy-start | bytes 580
  530.1 119.2 %copy-start.136 = (pred[192]{0:T(512)(128)(4,1)}, pred[192]{0:T(512)(128)(4,1)S(1)}, u32[]{:S(2)}) copy-start(pred[192]{0:T(512)(128)(4,1)S(1)} %get-tuple-element.132) | copy-start | bytes 580
  530.1 119.2 %copy-start.138 = (pred[192]{0:T(512)(128)(4,1)}, pred[192]{0:T(512)(128)(4,1)S(1)}, u32[]{:S(2)}) copy-start(pred[192]{0:T(512)(128)(4,1)S(1)} %get-tuple-element.133) | copy-start | bytes 580
  566.2 36.2 %collective-permute-start.10 = (bf16[128,6144]{1,0:T(8,128)(2,1)}, bf16[128,6144]{1,0:T(8,128)(2,1)S(1)}, u32[]{:S(2)}, u32[]{:S(2)}) collective-permute-start(bf16[128,6144]{1,0:T(8,128)(2,1)} %collective-permute-done.9), channel_id=1, source_target_pairs={{0,2},{2,4},{4,6},{6,8},{8,10},{10,12},{12,14},{14,16},{16,18},{18... | collective-permute-start | bytes 4718600 | tf_op jit(solution)/shard_map/ppermute | solution.py:166
  567.4 81.9 %copy-start.37 = (f32[4096]{0:T(1024)}, f32[4096]{0:T(1024)S(1)}, u32[]{:S(2)}) copy-start(f32[4096]{0:T(1024)S(1)} %get-tuple-element.25) | copy-start | bytes 49156
  568.0 81.2 %copy-start.25 = (f32[4096]{0:T(1024)}, f32[4096]{0:T(1024)S(1)}, u32[]{:S(2)}) copy-start(f32[4096]{0:T(1024)S(1)} %get-tuple-element.122) | copy-start | bytes 49156
  568.1 81.2 %copy-start.27 = (f32[4096]{0:T(1024)}, f32[4096]{0:T(1024)S(1)}, u32[]{:S(2)}) copy-start(f32[4096]{0:T(1024)S(1)} %get-tuple-element.123) | copy-start | bytes 49156
  568.1 81.2 %copy-start.29 = (f32[4096]{0:T(1024)}, f32[4096]{0:T(1024)S(1)}, u32[]{:S(2)}) copy-start(f32[4096]{0:T(1024)S(1)} %get-tuple-element.124) | copy-start | bytes 49156
  568.1 81.2 %copy-start.31 = (f32[4096]{0:T(1024)}, f32[4096]{0:T(1024)S(1)}, u32[]{:S(2)}) copy-start(f32[4096]{0:T(1024)S(1)} %get-tuple-element.125) | copy-start | bytes 49156
  568.1 81.3 %copy-start.33 = (f32[4096]{0:T(1024)}, f32[4096]{0:T(1024)S(1)}, u32[]{:S(2)}) copy-start(f32[4096]{0:T(1024)S(1)} %get-tuple-element.126) | copy-start | bytes 49156
  568.1 81.3 %copy-start.35 = (f32[4096]{0:T(1024)}, f32[4096]{0:T(1024)S(1)}, u32[]{:S(2)}) copy-start(f32[4096]{0:T(1024)S(1)} %get-tuple-element.127) | copy-start | bytes 49156
  568.1 108.0 %copy-start.65 = (f32[4096]{0:T(1024)}, f32[4096]{0:T(1024)S(1)}, u32[]{:S(2)}) copy-start(f32[4096]{0:T(1024)S(1)} %get-tuple-element.31) | copy-start | bytes 49156
  568.1 108.0 %copy-start.67 = (f32[4096]{0:T(1024)}, f32[4096]{0:T(1024)S(1)}, u32[]{:S(2)}) copy-start(f32[4096]{0:T(1024)S(1)} %get-tuple-element.32) | copy-start | bytes 49156
  603.7 35.2 %collective-permute-start.11 = (bf16[128,6144]{1,0:T(8,128)(2,1)S(1)}, bf16[128,6144]{1,0:T(8,128)(2,1)}, u32[]{:S(2)}, u32[]{:S(2)}) collective-permute-start(bf16[128,6144]{1,0:T(8,128)(2,1)S(1)} %collective-permute-done.10), channel_id=1, source_target_pairs={{0,2},{2,4},{4,6},{6,8},{8,10},{10,12},{12,14},{14,16},{16,18},{18... | collective-permute-start | bytes 4718600 | tf_op jit(solution)/shard_map/ppermute | solution.py:166
  638.9 34.7 %collective-permute-start.12 = (bf16[128,6144]{1,0:T(8,128)(2,1)}, bf16[128,6144]{1,0:T(8,128)(2,1)}, u32[]{:S(2)}, u32[]{:S(2)}) collective-permute-start(bf16[128,6144]{1,0:T(8,128)(2,1)} %collective-permute-done.11), channel_id=1, source_target_pairs={{0,2},{2,4},{4,6},{6,8},{8,10},{10,12},{12,14},{14,16},{16,18},{18... | collective-permute-start | bytes 4718600 | tf_op jit(solution)/shard_map/ppermute | solution.py:166
  673.6 34.8 %collective-permute-start.13 = (bf16[128,6144]{1,0:T(8,128)(2,1)}, bf16[128,6144]{1,0:T(8,128)(2,1)S(1)}, u32[]{:S(2)}, u32[]{:S(2)}) collective-permute-start(bf16[128,6144]{1,0:T(8,128)(2,1)} %collective-permute-done.12), channel_id=1, source_target_pairs={{0,2},{2,4},{4,6},{6,8},{8,10},{10,12},{12,14},{14,16},{16,18},{18... | collective-permute-start | bytes 4718600 | tf_op jit(solution)/shard_map/ppermute | solution.py:166
  674.7 102.6 %copy-start.43 = (f32[1,4096]{1,0:T(1,128)}, f32[1,4096]{1,0:T(1,128)S(1)}, u32[]{:S(2)}) copy-start(f32[1,4096]{1,0:T(1,128)S(1)} %get-tuple-element.14) | copy-start | bytes 49156
  674.7 102.6 %copy-start.45 = (f32[1,4096]{1,0:T(1,128)}, f32[1,4096]{1,0:T(1,128)S(1)}, u32[]{:S(2)}) copy-start(f32[1,4096]{1,0:T(1,128)S(1)} %get-tuple-element.15) | copy-start | bytes 49156
  674.7 102.6 %copy-start.49 = (f32[1,4096]{1,0:T(1,128)}, f32[1,4096]{1,0:T(1,128)S(1)}, u32[]{:S(2)}) copy-start(f32[1,4096]{1,0:T(1,128)S(1)} %get-tuple-element.13) | copy-start | bytes 49156
  674.7 102.6 %copy-start.57 = (f32[1,4096]{1,0:T(1,128)}, f32[1,4096]{1,0:T(1,128)S(1)}, u32[]{:S(2)}) copy-start(f32[1,4096]{1,0:T(1,128)S(1)} %get-tuple-element.16) | copy-start | bytes 49156
  674.7 102.6 %copy-start.59 = (f32[1,4096]{1,0:T(1,128)}, f32[1,4096]{1,0:T(1,128)S(1)}, u32[]{:S(2)}) copy-start(f32[1,4096]{1,0:T(1,128)S(1)} %get-tuple-element.17) | copy-start | bytes 49156
  674.7 102.6 %copy-start.61 = (f32[1,4096]{1,0:T(1,128)}, f32[1,4096]{1,0:T(1,128)S(1)}, u32[]{:S(2)}) copy-start(f32[1,4096]{1,0:T(1,128)S(1)} %get-tuple-element.18) | copy-start | bytes 49156
  674.7 102.6 %copy-start.63 = (f32[1,4096]{1,0:T(1,128)}, f32[1,4096]{1,0:T(1,128)S(1)}, u32[]{:S(2)}) copy-start(f32[1,4096]{1,0:T(1,128)S(1)} %get-tuple-element.19) | copy-start | bytes 49156
  674.7 102.6 %copy-start.53 = (f32[4096]{0:T(1024)}, f32[4096]{0:T(1024)S(1)}, u32[]{:S(2)}) copy-start(f32[4096]{0:T(1024)S(1)} %get-tuple-element.94) | copy-start | bytes 49156
  674.8 102.6 %copy-start.55 = (f32[4096]{0:T(1024)}, f32[4096]{0:T(1024)S(1)}, u32[]{:S(2)}) copy-start(f32[4096]{0:T(1024)S(1)} %get-tuple-element.95) | copy-start | bytes 49156
  708.4 34.4 %collective-permute-start.14 = (bf16[128,6144]{1,0:T(8,128)(2,1)S(1)}, bf16[128,6144]{1,0:T(8,128)(2,1)S(1)}, u32[]{:S(2)}, u32[]{:S(2)}) collective-permute-start(bf16[128,6144]{1,0:T(8,128)(2,1)S(1)} %collective-permute-done.13), channel_id=1, source_target_pairs={{0,2},{2,4},{4,6},{6,8},{8,10},{10,12},{12,14},{14,16},{16,18},{18... | collective-permute-start | bytes 4718600 | tf_op jit(solution)/shard_map/ppermute | solution.py:166
  742.8 31.9 %collective-permute-start.15 = (bf16[128,6144]{1,0:T(8,128)(2,1)S(1)}, bf16[128,6144]{1,0:T(8,128)(2,1)S(1)}, u32[]{:S(2)}, u32[]{:S(2)}) collective-permute-start(bf16[128,6144]{1,0:T(8,128)(2,1)S(1)} %collective-permute-done.14), channel_id=1, source_target_pairs={{0,2},{2,4},{4,6},{6,8},{8,10},{10,12},{12,14},{14,16},{16,18},{18... | collective-permute-start | bytes 4718600 | tf_op jit(solution)/shard_map/ppermute | solution.py:166
  841.4 119.7 %copy-start.21 = (f32[192,3072]{1,0:T(8,128)}, f32[192,3072]{1,0:T(8,128)S(1)}, u32[]{:S(2)}) copy-start(f32[192,3072]{1,0:T(8,128)S(1)} %fusion.52) | copy-start | bytes 7077892
  983.5 12.6 %collective-permute-start = (bf16[30,1024]{1,0:T(8,128)(2,1)S(1)}, bf16[30,1024]{1,0:T(8,128)(2,1)S(1)}, u32[]{:S(2)}, u32[]{:S(2)}) collective-permute-start(bf16[30,1024]{1,0:T(8,128)(2,1)S(1)} %slice.333), channel_id=1, source_target_pairs={{0,2},{2,4},{4,6},{6,8},{8,10},{10,12},{12,14},{14,16},{16,18},{18... | collective-permute-start | bytes 184328 | tf_op jit(solution)/shard_map/ppermute | solution.py:10
  (125 other events, 1945.7 us)
Sparse Core Ops, SparseCore 0:
  14.5 432.1 all-gather.3
